TPU v7x, 32 devices: a whole 2x2x4 slice. The times are simulated.
32 devices in a mesh: fs: 8 (over z, y), tp: 4 (over x, core).
Axes of the slice: x: 2, y: 2, z: 4, core: 2. Of those that a mesh axis runs over, the one named last changes fastest.
Arguments:
- tokens: bfloat16 [8192, 2048], P('fs'), may hold values from -6 to 6
- norm_gain: float32 [2048], P('fs'), may hold values from 0.1 to 1.9
- gate_train: float32 [8, 2048, 768], P(None, 'fs', 'tp'), may hold values from -0.125 to 0.125
- up_train: float32 [8, 2048, 768], P(None, 'fs', 'tp'), may hold values from -0.125 to 0.125
- down_train: float32 [8, 768, 2048], P(None, 'fs', 'tp'), may hold values from -0.21875 to 0.21875
- expert_ids: int32 [8192, 2], P('fs'), may hold values from 0 to 7, all different within a row; in each aligned block of 1024 rows (0 to 1023, 1024 to 2047, ...) at most 512 rows name the same one
- route_weights: float32 [8192, 2], P('fs'), may hold values from 0.1 to 1
Outputs:
- gate_serve: bfloat16 [8, 2048, 768], P('fs', None, 'tp')
- up_serve: bfloat16 [8, 2048, 768], P('fs', None, 'tp')
- down_serve: bfloat16 [8, 768, 2048], P('fs', 'tp')
- mixed: bfloat16 [8192, 2048], P('fs', 'tp')
Inputs may be any that keep to these rules, and one draw needn't show every extreme that they name: `expert_ids`: each row names 2 different experts. Within each aligned block of 1024 rows no expert is named more than 512 times, and in every block some expert is named exactly 512 times; every expert is named somewhere.
All inputs are finite; a program needn't handle non-finite values.
Results may differ from a plain program's by a relative error of at most 0.011.
Values may be sent and summed in bfloat16 or wider, within the bound.
A program may use at most 128 MiB of HBM per device.

v0:
```python
import jax
import jax.numpy as jnp
from jax import lax
from jax.sharding import PartitionSpec as P

epsilon = 1e-06


def on_device(tokens, norm_gain, gate_train, up_train, down_train, expert_ids, route_weights):
    experts, rows, cols = gate_train.shape
    fs_at = lax.axis_index("fs")
    tok_rows, picks = expert_ids.shape
    down_rows, down_cols = down_train.shape[1:]
    fs_count = lax.axis_size("fs")
    gate_up = jnp.concatenate(
        [norm_gain[None, :, None] * gate_train, norm_gain[None, :, None] * up_train], axis=2
    ).astype(jnp.bfloat16)
    gate_up = gate_up.transpose(1, 0, 2).reshape(rows, experts * 2 * cols)
    gate_up_all = lax.all_gather(gate_up, "fs", axis=0, tiled=True)
    down_all = lax.all_gather(
        down_train.astype(jnp.bfloat16).reshape(experts * down_rows, down_cols),
        "fs",
        axis=0,
        tiled=True,
    )
    tok_float = tokens.astype(jnp.float32)
    normed = (
        tok_float * lax.rsqrt(jnp.mean(tok_float * tok_float, axis=-1, keepdims=True) + epsilon)
    ).astype(jnp.bfloat16)
    shares = route_weights / jnp.sum(route_weights, axis=-1, keepdims=True)
    group = 2 * lax.axis_size("tp")
    picked = [jnp.zeros((tok_rows, cols), jnp.float32) for _ in range(picks)]
    for first in range(0, experts, group):
        part = gate_up_all[:, first * 2 * cols : (first + group) * 2 * cols]
        if first:
            part, picked = lax.optimization_barrier((part, picked))
        acts = jnp.dot(normed, part, preferred_element_type=jnp.float32)
        for at in range(group):
            g = acts[:, at * 2 * cols : at * 2 * cols + cols]
            u = acts[:, at * 2 * cols + cols : (at + 1) * 2 * cols]
            h = jax.nn.silu(g) * u
            for k in range(picks):
                picked[k] = picked[k] + jnp.where(expert_ids[:, k : k + 1] == first + at, h, 0.0)
    hidden = jnp.stack([picked[k] * shares[:, k : k + 1] for k in range(picks)], 0)
    hidden_all = lax.all_gather(hidden.astype(jnp.bfloat16), "tp", axis=2, tiled=True)
    hidden_all = hidden_all.reshape(picks, tok_rows, fs_count, 1, down_rows)
    ids = jnp.arange(experts, dtype=jnp.int32)[None, None, :, None]
    mixed = jnp.zeros((tok_rows, down_cols), jnp.float32)
    for first in range(0, fs_count, group):
        blocks = hidden_all[:, :, first : first + group]
        if first:
            blocks, mixed = lax.optimization_barrier((blocks, mixed))
        spread = jnp.zeros((tok_rows, group, experts, down_rows), jnp.bfloat16)
        for k in range(picks):
            spread = jnp.where(expert_ids[:, k][:, None, None, None] == ids, blocks[k], spread)
        depth = experts * down_rows
        mixed = mixed + jnp.dot(
            spread.reshape(tok_rows, group * depth),
            down_all[first * depth : (first + group) * depth],
            preferred_element_type=jnp.float32,
        )
    mixed = mixed.astype(jnp.bfloat16)
    own = lax.dynamic_slice_in_dim(gate_up_all, fs_at * 2 * cols, 2 * cols, 1)
    down_own = lax.dynamic_slice_in_dim(
        down_all.reshape(fs_count, experts, down_rows, down_cols), fs_at, 1, 1
    ).reshape(1, fs_count * down_rows, down_cols)
    down_serve = lax.all_to_all(down_own, "tp", split_axis=1, concat_axis=2, tiled=True)
    return (own[None, :, :cols], own[None, :, cols:], down_serve, mixed)


def solution(mesh):
    return jax.shard_map(
        on_device,
        mesh=mesh,
        in_specs=(
            P("fs", None),
            P("fs"),
            P(None, "fs", "tp"),
            P(None, "fs", "tp"),
            P(None, "fs", "tp"),
            P("fs", None),
            P("fs", None),
        ),
        out_specs=(P("fs", None, "tp"), P("fs", None, "tp"), P("fs", "tp", None), P("fs", "tp")),
        check_vma=False,
    )
```

profile of v0, /device:TPU:0, one launch (start us, length us, event | category | flops | bytes accessed | tf_op | source)
XLA Modules:
  0.0 353.5 jit_solution(751838854216082823)
XLA Ops:
  7.2 0.0 copy-start
  7.2 0.0 all-gather.4.cloned.1.call-start
  7.2 2.3 multiply_convert_fusion.1
  9.6 0.0 copy-start.2
  9.6 0.0 copy-start.1
  9.6 1.3 pad_maximum_fusion
  10.9 0.0 all-gather.4.cloned.1.call-update
  10.9 0.0 all-gather.6.cloned.1.call-start
  10.9 0.0 copy-done
  10.9 1.0 convert_element_type.14
  11.9 0.0 all-gather.6.cloned.1.call-update
  11.9 0.0 all-gather.8.cloned.1.call-start
  12.0 0.0 copy-done.2
  12.0 0.0 copy-done.1
  12.0 0.2 compare_reduce_fusion.15
  12.2 3.1 fusion
  15.4 174.5 %all-gather.4.cloned.1.call-done = bf16[2048,3072]{0,1:T(8,128)(2,1)} async-done(((bf16[256,3072]{0,1:T(8,128)(2,1)}), bf16[2048,3072]{0,1:T(8,128)(2,1)}) %all-gather.4.cloned.1.call-update) | async-done | bytes 12582928 | tf_op jit(solution)/shard_map/all_gather | solution.py:19
  189.9 17.1 %fusion.2 = f32[1024,3072]{1,0:T(8,128)S(1)} fusion(bf16[2048,3072]{0,1:T(8,128)(2,1)} %all-gather.4.cloned.1.call-done, bf16[1024,2048]{1,0:T(8,128)(2,1)} %param.7, f32[1024]{0:T(1024)S(1)} %add_rsqrt_fusion), kind=kOutput, calls=%fused_computation.5 | convolution fusion | flops 12891193344 | bytes 29364224 | tf_op jit(solution)/shard_map/dot_general | solution.py:37
  207.0 4.5 %fusion.5 = bf16[1,1024,192]{2,1,0:T(8,128)(2,1)S(1)} fusion(f32[1024]{0:T(1024)S(1)} %bitcast.47, pred[1024]{0:T(1024)(128)(4,1)S(1)} %get-tuple-element.19, pred[1024]{0:T(1024)(128)(4,1)S(1)} %get-tuple-element.18, pred[1024]{0:T(1024)(128)(4,1)S(1)} %get-tuple-element.17, pred[1024]{0:T(1024)(128)(4,1)S(1)} %get-tuple-element.16, ...), kind=kLoop, calls=%fused_computation.24 | loop fusion | flops 11206656 | bytes 12988416 | tf_op jit(solution)/shard_map/stack | solution.py:44
  211.5 4.5 %fusion.6 = bf16[1,1024,192]{2,1,0:T(8,128)(2,1)S(1)} fusion(f32[1024]{0:T(1024)S(1)} %bitcast.46, pred[1024]{0:T(1024)(128)(4,1)S(1)} %get-tuple-element.12, pred[1024]{0:T(1024)(128)(4,1)S(1)} %get-tuple-element.11, pred[1024]{0:T(1024)(128)(4,1)S(1)} %get-tuple-element.10, pred[1024]{0:T(1024)(128)(4,1)S(1)} %get-tuple-element.9, ...), kind=kLoop, calls=%fused_computation.25 | loop fusion | flops 11206656 | bytes 12988416 | tf_op jit(solution)/shard_map/stack | solution.py:44
  216.0 0.2 pad_maximum_fusion.1
  216.2 2.0 copy.22
  218.2 0.0 all-gather.8.cloned.1.call-update
  218.2 71.3 %all-gather.6.cloned.1.call-done = bf16[6144,512]{1,0:T(8,128)(2,1)} async-done(((bf16[768,512]{1,0:T(8,128)(2,1)}), bf16[6144,512]{1,0:T(8,128)(2,1)}) %all-gather.6.cloned.1.call-update) | async-done | bytes 6291472 | tf_op jit(solution)/shard_map/all_gather | solution.py:20
  289.5 1.2 constant_dynamic-slice_fusion
  290.8 1.2 copy.30
  292.0 0.5 broadcast.126
  292.5 5.4 %reduce.32 = bf16[768,512]{1,0:T(8,128)(2,1)S(1)} reduce(bf16[768,1,512]{2,1,0:T(2,128)(2,1)S(1)} %bitcast.37, bf16[]{:T(256)} %broadcast.126), dimensions={1}, to_apply=%bitcast.32.reduce_sub_computation | reduce | bytes 1572866
  297.9 1.4 reshape.117
  299.3 3.7 %all-to-all-start = ((bf16[4,2,49152]{2,1,0:T(2,128)(2,1)}), bf16[4,2,49152]{2,1,0:T(2,128)(2,1)S(1)}, u32[]{:S(2)}, u32[]{:S(2)}) async-start(bf16[4,2,49152]{2,1,0:T(2,128)(2,1)} %reshape.117), calls=%async_computation | async-start | bytes 1572864 | tf_op jit(solution)/shard_map/all_to_all | solution.py:67
  303.0 20.2 %all-to-all-done = bf16[4,2,49152]{2,1,0:T(2,128)(2,1)S(1)} async-done(((bf16[4,2,49152]{2,1,0:T(2,128)(2,1)}), bf16[4,2,49152]{2,1,0:T(2,128)(2,1)S(1)}, u32[]{:S(2)}, u32[]{:S(2)}) %all-to-all-start) | async-done | bytes 786464 | tf_op jit(solution)/shard_map/all_to_all | solution.py:67
  323.2 0.7 reshape.118
  324.0 0.2 copy.25
  324.2 1.0 copy.28
  325.2 2.7 dynamic-slice_bitcast_fusion
  327.9 0.0 all-gather.8.cloned.1.call-done
  327.9 7.8 %fusion.7 = (bf16[1,1024,768]{1,0,2:T(2,128)(2,1)S(1)}, bf16[1,1024,768]{1,0,2:T(2,128)(2,1)S(1)}) fusion(bf16[2,1024,768]{1,0,2:T(2,128)(2,1)} %all-gather.8.cloned.1.call-done), kind=kLoop, calls=%fused_computation.47 | loop fusion | bytes 6291456 | tf_op jit(solution)/shard_map/slice | solution.py:55
  335.7 0.6 copy.26
  336.3 0.0 slice-start
  336.3 0.6 copy.27
  336.9 0.0 slice-start.1
  336.9 1.9 select_select_fusion
  338.8 0.0 slice-done
  338.8 0.5 slice-done.1
  339.3 7.6 %convolution_convert_fusion = bf16[1024,512]{1,0:T(8,128)(2,1)} fusion(bf16[1024,6144]{0,1:T(8,128)(2,1)S(1)} %bitcast.33, bf16[6144,512]{1,0:T(8,128)(2,1)S(1)} %bitcast.45), kind=kOutput, calls=%fused_computation.10 | convolution fusion | flops 6442975232 | bytes 19922944 | tf_op jit(solution)/shard_map/dot_general | solution.py:57
  (7 shorter events, 0.1 us)
Async XLA Ops:
  7.2 3.8 %copy-start = (f32[8,96,512]{2,1,0:T(8,128)S(1)}, f32[8,96,512]{2,1,0:T(8,128)}, u32[]{:S(2)}) copy-start(f32[8,96,512]{2,1,0:T(8,128)} %param.11) | copy-start | bytes 4718596
  7.2 182.7 %all-gather.4.cloned.1.call-start = ((), (), s32[]{:S(2)}) async-start(), calls=%async_computation.1 | async-start | bytes 14155776 | tf_op jit(solution)/shard_map/all_gather | solution.py:19
  9.6 2.4 copy-start.2
  9.6 2.5 copy-start.1
  10.9 278.7 %all-gather.6.cloned.1.call-start = ((), (), s32[]{:S(2)}) async-start(), calls=%async_computation.2 | async-start | bytes 7077888 | tf_op jit(solution)/shard_map/all_gather | solution.py:20
  11.9 315.9 %all-gather.8.cloned.1.call-start = ((), (), s32[]{:S(2)}) async-start(), calls=%async_computation.3 | async-start | bytes 3932160 | tf_op jit(solution)/shard_map/all_gather | solution.py:45
  299.3 23.9 %all-to-all-start = ((bf16[4,2,49152]{2,1,0:T(2,128)(2,1)}), bf16[4,2,49152]{2,1,0:T(2,128)(2,1)S(1)}, u32[]{:S(2)}, u32[]{:S(2)}) async-start(bf16[4,2,49152]{2,1,0:T(2,128)(2,1)} %reshape.117), calls=%async_computation | async-start | bytes 1572864 | tf_op jit(solution)/shard_map/all_to_all | solution.py:67
  336.3 2.5 slice-start
  336.9 2.4 slice-start.1
Sparse Core Ops, SparseCore 0:
  11.0 178.8 all-gather.3
  192.6 96.8 all-gather.5
  291.7 35.1 all-gather.7
where the time goes:
time: 354 us; the launch traced here: 353 us
  waiting for transfers between devices  266 us (75%)
  matrix products  24.7 us (7%)
  other arithmetic  24.4 us (7%)
  local copies, waits for them, and re-layouts  20.5 us (6%)
  between operations  14 us (4%)
  starting transfers between devices  3.8 us (1%)
    all_gather x1, waiting for transfers between devices, on_device(): gate_up_all = lax.all_gather(gate_up, 'fs', axis=0, tiled=True)  175 us
    all_gather x1, waiting for transfers between devices, on_device(): lax.all_gather(down_train.astype(jnp.bfloat16).reshape(experts * down_row...  71.3 us
    all_to_all x1, waiting for transfers between devices, on_device(): lax.all_to_all(down_own, 'tp', split_axis=1, concat_axis=2, tiled=True)  20.2 us
    dot_general x1, matrix products, on_device(): acts = jnp.dot(normed, part, preferred_element_type=jnp.float32)  17.1 us
    another operation x3, other arithmetic, on_device(): jnp.stack([picked[k] * shares[:, k:k + 1] for k in range(picks)], 0)  9.18 us
    slice x1, local copies, waits for them, and re-layouts, on_device(): blocks[k]  7.82 us
    dot_general x1, matrix products, on_device(): jnp.dot(spread.reshape(tok_rows, group * depth), down_all[first * depth:(...  7.64 us
  transfers between devices with their start and end apart: 4, of which 3 were waited for; matrix products, arithmetic and copies ran while one was open for 13% of the time, Pallas kernels for 0%

commit v1 on v0

--- a/solution.py
+++ b/solution.py
@@ -64,7 +64,10 @@
     down_own = lax.dynamic_slice_in_dim(
         down_all.reshape(fs_count, experts, down_rows, down_cols), fs_at, 1, 1
     ).reshape(1, fs_count * down_rows, down_cols)
-    down_serve = lax.all_to_all(down_own, "tp", split_axis=1, concat_axis=2, tiled=True)
+    down_serve = jnp.concatenate(
+        lax.all_to_all(jnp.stack(jnp.split(down_own, lax.axis_size("tp"), axis=1)), "tp", 0, 0),
+        axis=2,
+    )
     return (own[None, :, :cols], own[None, :, cols:], down_serve, mixed)
 
 

time: 354 us -> 351 us (level)
  waiting for transfers between devices: 266 us -> 272 us
  other arithmetic: 24.4 us -> 19.9 us
  local copies, waits for them, and re-layouts: 20.5 us -> 16.5 us
    all_gather x1, waiting for transfers between devices: 0.01 us -> 7.35 us  [on_device(): lax.all_gather(hidden.astype(jnp.bfloat16), 'tp', axis=2, tiled=True)]
    unnamed x2 -> x1, other arithmetic: 5.43 us -> 0.01 us
  transfers between devices with their start and end apart: 4 -> 4, of which waited for: 3 -> 4; matrix products, arithmetic and copies ran while one was open for 13% -> 11% of each run, Pallas kernels for 0% -> 0%
where the time goes in v1:
time: 351 us
  waiting for transfers between devices  272 us (77%)
  matrix products  24.7 us (7%)
  other arithmetic  19.9 us (6%)
  local copies, waits for them, and re-layouts  16.5 us (5%)
  between operations  14 us (4%)
  starting transfers between devices  3.8 us (1%)
    all_gather x1, waiting for transfers between devices, on_device(): gate_up_all = lax.all_gather(gate_up, 'fs', axis=0, tiled=True)  175 us
    all_gather x1, waiting for transfers between devices, on_device(): lax.all_gather(down_train.astype(jnp.bfloat16).reshape(experts * down_row...  71.3 us
    all_to_all x1, waiting for transfers between devices, on_device(): lax.all_to_all(jnp.stack(jnp.split(down_own, lax.axis_size('tp'), axis=1)...  18.8 us
    dot_general x1, matrix products, on_device(): acts = jnp.dot(normed, part, preferred_element_type=jnp.float32)  17.1 us
    another operation x3, other arithmetic, on_device(): jnp.stack([picked[k] * shares[:, k:k + 1] for k in range(picks)], 0)  9.18 us
    slice x1, local copies, waits for them, and re-layouts, on_device(): blocks[k]  7.82 us
    dot_general x1, matrix products, on_device(): jnp.dot(spread.reshape(tok_rows, group * depth), down_all[first * depth:(...  7.65 us
    all_gather x1, waiting for transfers between devices, on_device(): lax.all_gather(hidden.astype(jnp.bfloat16), 'tp', axis=2, tiled=True)  7.35 us
  transfers between devices with their start and end apart: 4, of which 4 were waited for; matrix products, arithmetic and copies ran while one was open for 11% of the time, Pallas kernels for 0%

profile of v1, /device:TPU:0, one launch (start us, length us, event | category | flops | bytes accessed | tf_op | source)
XLA Modules:
  0.0 350.9 jit_solution(14751124145734465730)
XLA Ops:
  7.2 0.0 copy-start
  7.2 0.0 all-gather.4.cloned.1.call-start
  7.2 2.3 multiply_convert_fusion.1
  9.6 0.0 copy-start.2
  9.6 0.0 copy-start.1
  9.6 1.3 pad_maximum_fusion
  10.9 0.0 all-gather.4.cloned.1.call-update
  10.9 0.0 all-gather.6.cloned.1.call-start
  10.9 0.0 copy-done
  10.9 1.0 convert_element_type.14
  11.9 0.0 all-gather.6.cloned.1.call-update
  11.9 0.0 all-gather.8.cloned.1.call-start
  12.0 0.0 copy-done.2
  12.0 0.0 copy-done.1
  12.0 0.2 compare_reduce_fusion.15
  12.2 3.1 fusion
  15.4 174.5 %all-gather.4.cloned.1.call-done = bf16[2048,3072]{0,1:T(8,128)(2,1)} async-done(((bf16[256,3072]{0,1:T(8,128)(2,1)}), bf16[2048,3072]{0,1:T(8,128)(2,1)}) %all-gather.4.cloned.1.call-update) | async-done | bytes 12582928 | tf_op jit(solution)/shard_map/all_gather | solution.py:19
  189.9 17.1 %fusion.2 = f32[1024,3072]{1,0:T(8,128)S(1)} fusion(bf16[2048,3072]{0,1:T(8,128)(2,1)} %all-gather.4.cloned.1.call-done, bf16[1024,2048]{1,0:T(8,128)(2,1)} %param.7, f32[1024]{0:T(1024)S(1)} %add_rsqrt_fusion), kind=kOutput, calls=%fused_computation.5 | convolution fusion | flops 12891193344 | bytes 29364224 | tf_op jit(solution)/shard_map/dot_general | solution.py:37
  207.0 4.5 %fusion.5 = bf16[1,1024,192]{2,1,0:T(8,128)(2,1)S(1)} fusion(f32[1024]{0:T(1024)S(1)} %bitcast.47, pred[1024]{0:T(1024)(128)(4,1)S(1)} %get-tuple-element.19, pred[1024]{0:T(1024)(128)(4,1)S(1)} %get-tuple-element.18, pred[1024]{0:T(1024)(128)(4,1)S(1)} %get-tuple-element.17, pred[1024]{0:T(1024)(128)(4,1)S(1)} %get-tuple-element.16, ...), kind=kLoop, calls=%fused_computation.25 | loop fusion | flops 11206656 | bytes 12988416 | tf_op jit(solution)/shard_map/stack | solution.py:44
  211.5 4.5 %fusion.6 = bf16[1,1024,192]{2,1,0:T(8,128)(2,1)S(1)} fusion(f32[1024]{0:T(1024)S(1)} %bitcast.46, pred[1024]{0:T(1024)(128)(4,1)S(1)} %get-tuple-element.12, pred[1024]{0:T(1024)(128)(4,1)S(1)} %get-tuple-element.11, pred[1024]{0:T(1024)(128)(4,1)S(1)} %get-tuple-element.10, pred[1024]{0:T(1024)(128)(4,1)S(1)} %get-tuple-element.9, ...), kind=kLoop, calls=%fused_computation.26 | loop fusion | flops 11206656 | bytes 12988416 | tf_op jit(solution)/shard_map/stack | solution.py:44
  216.0 0.2 pad_maximum_fusion.1
  216.2 2.0 copy.21
  218.2 0.0 all-gather.8.cloned.1.call-update
  218.2 71.3 %all-gather.6.cloned.1.call-done = bf16[6144,512]{1,0:T(8,128)(2,1)} async-done(((bf16[768,512]{1,0:T(8,128)(2,1)}), bf16[6144,512]{1,0:T(8,128)(2,1)}) %all-gather.6.cloned.1.call-update) | async-done | bytes 6291472 | tf_op jit(solution)/shard_map/all_gather | solution.py:20
  289.5 1.2 constant_dynamic-slice_fusion
  290.7 0.1 slice_bitcast_fusion.3
  290.8 1.0 pad_maximum_fusion.2
  291.8 3.7 %all-to-all-start = ((bf16[4,1,192,512]{3,2,1,0:T(8,128)(2,1)}), bf16[4,1,192,512]{3,2,1,0:T(8,128)(2,1)S(1)}, u32[]{:S(2)}, u32[]{:S(2)}) async-start(bf16[4,1,192,512]{3,2,1,0:T(8,128)(2,1)} %pad_maximum_fusion.2), calls=%async_computation | async-start | bytes 1572864 | tf_op jit(solution)/shard_map/all_to_all | solution.py:68
  295.5 18.8 %all-to-all-done = bf16[4,1,192,512]{3,2,1,0:T(8,128)(2,1)S(1)} async-done(((bf16[4,1,192,512]{3,2,1,0:T(8,128)(2,1)}), bf16[4,1,192,512]{3,2,1,0:T(8,128)(2,1)S(1)}, u32[]{:S(2)}, u32[]{:S(2)}) %all-to-all-start) | async-done | bytes 786464 | tf_op jit(solution)/shard_map/all_to_all | solution.py:68
  314.3 1.0 copy.26
  315.2 2.7 dynamic-slice_bitcast_fusion
  317.9 7.4 %all-gather.8.cloned.1.call-done = bf16[2,1024,768]{1,0,2:T(2,128)(2,1)} async-done(((bf16[2,1024,192]{1,0,2:T(2,128)(2,1)}), bf16[2,1024,768]{1,0,2:T(2,128)(2,1)}) %all-gather.8.cloned.1.call-update) | async-done | bytes 3145744 | tf_op jit(solution)/shard_map/all_gather | solution.py:45
  325.3 7.8 %fusion.7 = (bf16[1,1024,768]{1,0,2:T(2,128)(2,1)S(1)}, bf16[1,1024,768]{1,0,2:T(2,128)(2,1)S(1)}) fusion(bf16[2,1024,768]{1,0,2:T(2,128)(2,1)} %all-gather.8.cloned.1.call-done), kind=kLoop, calls=%fused_computation.52 | loop fusion | bytes 6291456 | tf_op jit(solution)/shard_map/slice | solution.py:55
  333.1 0.6 copy.24
  333.7 0.0 slice-start
  333.7 0.6 copy.25
  334.3 0.0 slice-start.1
  334.3 1.9 select_select_fusion
  336.2 0.0 slice-done
  336.2 0.5 slice-done.1
  336.7 7.6 %convolution_convert_fusion = bf16[1024,512]{1,0:T(8,128)(2,1)} fusion(bf16[1024,6144]{0,1:T(8,128)(2,1)S(1)} %bitcast.35, bf16[6144,512]{1,0:T(8,128)(2,1)S(1)} %bitcast.45), kind=kOutput, calls=%fused_computation.10 | convolution fusion | flops 6442975232 | bytes 19922944 | tf_op jit(solution)/shard_map/dot_general | solution.py:57
  (7 shorter events, 0.1 us)
Async XLA Ops:
  7.2 3.8 %copy-start = (f32[8,96,512]{2,1,0:T(8,128)S(1)}, f32[8,96,512]{2,1,0:T(8,128)}, u32[]{:S(2)}) copy-start(f32[8,96,512]{2,1,0:T(8,128)} %param.11) | copy-start | bytes 4718596
  7.2 182.7 %all-gather.4.cloned.1.call-start = ((), (), s32[]{:S(2)}) async-start(), calls=%async_computation.1 | async-start | bytes 14155776 | tf_op jit(solution)/shard_map/all_gather | solution.py:19
  9.6 2.4 copy-start.2
  9.6 2.5 copy-start.1
  10.9 278.7 %all-gather.6.cloned.1.call-start = ((), (), s32[]{:S(2)}) async-start(), calls=%async_computation.2 | async-start | bytes 7077888 | tf_op jit(solution)/shard_map/all_gather | solution.py:20
  11.9 313.3 %all-gather.8.cloned.1.call-start = ((), (), s32[]{:S(2)}) async-start(), calls=%async_computation.3 | async-start | bytes 3932160 | tf_op jit(solution)/shard_map/all_gather | solution.py:45
  291.8 22.5 %all-to-all-start = ((bf16[4,1,192,512]{3,2,1,0:T(8,128)(2,1)}), bf16[4,1,192,512]{3,2,1,0:T(8,128)(2,1)S(1)}, u32[]{:S(2)}, u32[]{:S(2)}) async-start(bf16[4,1,192,512]{3,2,1,0:T(8,128)(2,1)} %pad_maximum_fusion.2), calls=%async_computation | async-start | bytes 1572864 | tf_op jit(solution)/shard_map/all_to_all | solution.py:68
  333.7 2.5 slice-start
  334.3 2.4 slice-start.1
Sparse Core Ops, SparseCore 0:
  11.0 178.8 all-gather.3
  192.6 96.8 all-gather.5
  291.7 33.5 all-gather.7
